TPU v7x, 32 devices: a whole 2x2x4 slice. The times are simulated.
32 devices in a mesh: sp: 8 (over z, y), tp: 4 (over x, core).
Axes of the slice: x: 2, y: 2, z: 4, core: 2. Of those that a mesh axis runs over, the one named last changes fastest.
Arguments:
- queries: bfloat16 [8192, 1024], P('sp', 'tp'), may hold values from -6 to 6
- keys: bfloat16 [8192, 1024], P('sp', 'tp'), may hold values from -6 to 6
- values: bfloat16 [8192, 1024], P('sp', 'tp'), may hold values from -6 to 6
- gates: bfloat16 [8192, 1024], P('sp', 'tp'), may hold values from -6 to 6
- log_decay: float32 [8192, 8], P('sp', 'tp'), may hold values from -1.6 to 0, as said below
- norm_gain: float32 [8, 128], P('tp'), may hold values from 0.1 to 1.9
- out_weight: bfloat16 [1024, 2048], P('tp'), may hold values from -0.1875 to 0.1875
- resid: bfloat16 [8192, 2048], P(('sp', 'tp')), may hold values from -6 to 6
- post_mix_gain: float32 [2048], replicated, may hold values from 0.1 to 1.9
- pre_ffn_gain: float32 [2048], replicated, may hold values from 0.1 to 1.9
- w_gate: bfloat16 [2048, 5632], P('sp', 'tp'), may hold values from -0.125 to 0.125
- w_up: bfloat16 [2048, 5632], P('sp', 'tp'), may hold values from -0.125 to 0.125
- w_down: bfloat16 [5632, 2048], P('tp', 'sp'), may hold values from -0.078125 to 0.078125
- post_ffn_gain: float32 [2048], replicated, may hold values from 0.1 to 1.9
Outputs:
- updated: bfloat16 [8192, 2048], P(('sp', 'tp'))
Inputs may be any that keep to these rules, and one draw needn't show every extreme that they name: `log_decay`: every entry is negative.
All inputs are finite; a program needn't handle non-finite values.
Results may differ from a plain program's by a relative error of at most 0.02.
Values may be sent and summed in bfloat16 or wider, within the bound.
A program may use at most 128 MiB of HBM per device.

v0:
```python
import jax
import jax.numpy as jnp
from jax import lax
from jax.sharding import PartitionSpec as P

BLOCK = 512
EPSILON = 1e-06


def entering(x, axis, join, neutral):
    place = lax.axis_index(axis)
    gathered = jax.tree.map(
        lambda a, kind: lax.all_gather(a.astype(kind), axis), x, (jnp.bfloat16, jnp.bfloat16)
    )
    state = jax.tree.map(lambda a, e: jnp.zeros_like(a) + jnp.asarray(e, a.dtype), x, neutral)

    def one(step, state):
        return join(
            state,
            jax.tree.map(
                lambda a, own: lax.dynamic_index_in_dim(a, step, 0, False).astype(own.dtype),
                gathered,
                x,
            ),
        )

    return lax.fori_loop(0, place, one, state)


def rms_norm(values_in, gain_vec):
    widened = values_in.astype(jnp.float32)
    return (
        widened
        * lax.rsqrt(jnp.mean(widened * widened, axis=-1, keepdims=True) + EPSILON)
        * gain_vec
    )


def block_step(carried, pieces):
    query_blk, key_blk, value_blk, decay_blk = pieces
    length = query_blk.shape[1]
    key_scale = query_blk.shape[2] ** (-0.5)
    cumulative = jnp.cumsum(decay_blk, axis=1)
    log_gap = cumulative[:, :, None] - cumulative[:, None, :]
    causal = lax.broadcasted_iota(jnp.int32, (length, length), 0) >= lax.broadcasted_iota(
        jnp.int32, (length, length), 1
    )
    weight = jnp.where(causal[None], jnp.exp(jnp.minimum(log_gap, 0.0)), 0.0)
    products = jnp.einsum("htd,hsd->hts", query_blk, key_blk, preferred_element_type=jnp.float32)
    scores = (products * key_scale * weight).astype(jnp.bfloat16)
    within = jnp.einsum("hts,hsd->htd", scores, value_blk, preferred_element_type=jnp.float32)
    carried_term = (
        jnp.einsum(
            "htd,hde->hte", query_blk.astype(jnp.float32), carried, precision=lax.Precision.HIGHEST
        )
        * jnp.exp(cumulative)[:, :, None]
    )
    to_end = jnp.exp(cumulative[:, -1:] - cumulative) * key_scale
    scaled_keys = (key_blk.astype(jnp.float32) * to_end[:, :, None]).astype(jnp.bfloat16)
    added = jnp.einsum("hsd,hse->hde", scaled_keys, value_blk, preferred_element_type=jnp.float32)
    carried = jnp.exp(cumulative[:, -1])[:, None, None] * carried + added
    return (carried, within + carried_term)


def to_blocks(matrix, block_len, head_count):
    row_count = matrix.shape[0]
    return matrix.reshape(row_count // block_len, block_len, head_count, -1).transpose(0, 2, 1, 3)


def finish_heads(retention, gates, norm_gain):
    centered = retention - jnp.mean(retention, axis=-1, keepdims=True)
    variance = jnp.mean(centered * centered, axis=-1, keepdims=True)
    normed = centered * lax.rsqrt(variance + EPSILON) * norm_gain[None]
    gate_vals = gates.astype(jnp.float32).reshape(normed.shape)
    return (jax.nn.silu(gate_vals) * normed).reshape(normed.shape[0], -1).astype(jnp.bfloat16)


def combine_states(earlier, later):
    return (earlier[0] * later[0], later[0][:, None, None] * earlier[1] + later[1])


def per_device(
    queries,
    keys,
    values,
    gates,
    log_decay,
    norm_gain,
    out_weight,
    resid,
    post_mix_gain,
    pre_ffn_gain,
    w_gate,
    w_up,
    w_down,
    post_ffn_gain,
):
    row_count = queries.shape[0]
    head_count = log_decay.shape[1]
    head_dim = queries.shape[1] // head_count
    block_count = row_count // BLOCK
    query_blocks = to_blocks(queries, BLOCK, head_count)
    key_blocks = to_blocks(keys, BLOCK, head_count)
    value_blocks = to_blocks(values, BLOCK, head_count)
    decay_blocks = log_decay.reshape(block_count, BLOCK, head_count).transpose(0, 2, 1)
    start_state = jnp.zeros((head_count, head_dim, head_dim), jnp.float32)
    local_state, outputs = lax.scan(
        block_step, start_state, (query_blocks, key_blocks, value_blocks, decay_blocks)
    )
    retention = outputs.transpose(0, 2, 1, 3).reshape(row_count, head_count, head_dim)
    cumulative = jnp.cumsum(log_decay, axis=0)
    local_decay = jnp.exp(cumulative[-1])
    identity = (jnp.ones_like(local_decay), jnp.zeros_like(local_state))
    incoming = entering((local_decay, local_state), "sp", combine_states, identity)
    query_rows = queries.reshape(row_count, head_count, head_dim).astype(jnp.float32)
    retention = (
        retention
        + jnp.einsum("thd,hde->the", query_rows, incoming[1], precision=lax.Precision.HIGHEST)
        * jnp.exp(cumulative)[:, :, None]
    )
    retained = finish_heads(retention, gates, norm_gain)
    quarter = resid.shape[0]
    regrouped = lax.all_to_all(retained, "tp", split_axis=0, concat_axis=1, tiled=True)
    group_rows = out_weight.shape[0]
    empty_mix = jnp.zeros((quarter, out_weight.shape[1]), jnp.float32)
    running = empty_mix
    shard_piece = lax.all_gather(out_weight, "tp", axis=0, tiled=True)
    for offset in range(shard_piece.shape[0] // group_rows):
        columns = lax.dynamic_slice_in_dim(regrouped, offset * group_rows, group_rows, 1)
        part = jnp.dot(
            columns,
            shard_piece[offset * group_rows : (offset + 1) * group_rows],
            preferred_element_type=jnp.float32,
        )
        running = running + part.astype(jnp.bfloat16).astype(jnp.float32)
    mixed = running
    mixed = mixed.astype(jnp.bfloat16)
    middle = (resid.astype(jnp.float32) + rms_norm(mixed, post_mix_gain)).astype(jnp.bfloat16)
    ffn_input = rms_norm(middle, pre_ffn_gain).astype(jnp.bfloat16)
    gathered = lax.all_gather(ffn_input, "tp", axis=0, tiled=True)
    columns = gathered
    gate_act = jnp.dot(
        columns,
        lax.all_gather(w_gate, "sp", axis=0, tiled=True),
        preferred_element_type=jnp.float32,
    )
    up_act = jnp.dot(
        columns, lax.all_gather(w_up, "sp", axis=0, tiled=True), preferred_element_type=jnp.float32
    )
    down_full = lax.all_gather(w_down, "sp", axis=1, tiled=True)
    hidden = (jax.nn.silu(gate_act) * up_act).astype(jnp.bfloat16)
    branch = lax.psum_scatter(
        jnp.dot(hidden, down_full, preferred_element_type=jnp.float32)
        .astype(jnp.bfloat16)
        .astype(jnp.float32)
        .astype(jnp.bfloat16),
        "tp",
        scatter_dimension=0,
        tiled=True,
    )
    return (middle.astype(jnp.float32) + rms_norm(branch, post_ffn_gain)).astype(jnp.bfloat16)


def solution(mesh):
    in_specs = (
        P("sp", "tp"),
        P("sp", "tp"),
        P("sp", "tp"),
        P("sp", "tp"),
        P("sp", "tp"),
        P("tp", None),
        P("tp", None),
        P(("sp", "tp"), None),
        P(),
        P(),
        P("sp", "tp"),
        P("sp", "tp"),
        P("tp", "sp"),
        P(),
    )
    out_specs = P(("sp", "tp"), None)
    return jax.shard_map(
        per_device, mesh=mesh, in_specs=in_specs, out_specs=out_specs, check_vma=False
    )
```

profile of v0, /device:TPU:0, one launch (start us, length us, event | category | flops | bytes accessed | tf_op | source)
XLA Modules:
  0.0 438.4 jit_solution(6785753459974340258)
XLA Ops:
  6.5 0.7 all-gather.8.cloned.1.call-update
  7.3 0.7 all-gather.12.cloned.1.call-update
  8.1 0.7 copy.104
  8.8 0.6 reduce-window.16
  9.4 0.2 slice_reduce_fusion.1
  9.5 0.2 reduce-window.17
  9.7 0.1 add_bitcast_fusion.1
  9.8 0.2 fusion.48
  10.0 22.3 %all-gather.1 = bf16[8,1,2]{2,1,0:T(2,128)(2,1)S(1)} all-gather(bf16[1,1,2]{2,1,0:T(2,128)(2,1)S(1)} %bitcast.154), channel_id=1, replica_groups=mesh['sp'=8,'tp'=4] {'sp'}, dimensions={0}, use_global_device_ids=true | all-gather | bytes 36 | tf_op jit(solution)/shard_map/all_gather | solution.py:13
  32.3 0.1 copy.58
  32.4 0.1 reshape.172
  32.5 0.1 reshape.173
  32.7 0.1 reshape.174
  32.8 9.6 %while.26 = (s32[]{:T(128)}, f32[2,128,128]{2,1,0:T(8,128)S(1)}, f32[2,2,512,128]{3,2,1,0:T(8,128)}, f32[2,2,512]{2,1,0:T(2,128)S(1)}, bf16[2,2,512,128]{3,1,2,0...) while((s32[]{:T(128)}, f32[2,128,128]{2,1,0:T(8,128)S(1)}, ...), condition=%wide.region_3.4_spmd.clone, body=%wide.region_0.3_spmd.clone.sunk | while | flops 507643936 | bytes 5702508 | solution.py:107
  32.8 0.6 reduce-window.26
  33.5 0.2 slice_reduce_fusion.3
  33.6 0.2 reduce-window.27
  33.9 0.4 constant_dynamic-slice_fusion.12
  34.3 0.2 constant_dynamic-slice_fusion.11
  34.4 0.1 iota_compare_fusion.2
  34.5 1.0 fusion.75
  35.7 0.1 copy.124
  35.8 0.1 fusion.74
  35.8 1.2 fusion.76
  37.0 0.5 convolution_add_fusion.2
  37.6 0.6 reduce-window.26
  38.2 0.2 slice_reduce_fusion.3
  38.4 0.2 reduce-window.27
  38.7 0.4 constant_dynamic-slice_fusion.12
  39.0 0.2 constant_dynamic-slice_fusion.11
  39.2 0.1 iota_compare_fusion.2
  39.3 1.0 fusion.75
  40.4 0.1 copy.124
  40.5 0.1 fusion.74
  40.6 1.2 fusion.76
  41.8 0.5 convolution_add_fusion.2
  42.4 1.6 copy.57
  44.1 0.9 reshape.175
  45.0 0.2 copy.53
  45.2 33.1 %all-gather = bf16[16,128,128]{2,1,0:T(8,128)(2,1)S(1)} all-gather(bf16[2,128,128]{2,1,0:T(8,128)(2,1)S(1)} %convert_element_type.103), channel_id=2, replica_groups=mesh['sp'=8,'tp'=4] {'sp'}, dimensions={0}, use_global_device_ids=true | all-gather | bytes 589824 | tf_op jit(solution)/shard_map/all_gather | solution.py:13
  78.4 0.7 fusion.51
  79.1 0.1 multiply_reduce_fusion
  79.3 0.4 multiply_convert_fusion.4
  79.7 0.4 convert_element_type.105
  80.1 11.4 %all_to_all.16 = bf16[4,256,256]{1,2,0:T(8,128)(2,1)S(1)} all-to-all(bf16[4,256,256]{1,2,0:T(8,128)(2,1)S(1)} %copy.62), channel_id=1, replica_groups=mesh['sp'=8,'tp'=4] {'tp'}, dimensions={0} | all-to-all | bytes 1048576 | tf_op jit(solution)/shard_map/all_to_all | solution.py:123
  91.5 1.8 fusion.22
  93.4 1.7 fusion.23
  95.1 0.5 fusion.24
  95.6 0.8 fusion.25
  96.4 0.4 copy-done.3
  96.8 0.6 fusion.31
  97.4 1.3 fusion.33
  98.8 0.5 all-gather.14.cloned.1.call-update
  99.4 0.5 all-gather.16.cloned.1.call-update
  99.9 0.2 reduce-scatter.2.cloned.1.call-start
  100.1 41.9 %all-gather.12.cloned.1.call-done = bf16[2048,1408]{1,0:T(8,128)(2,1)} async-done(((bf16[256,1408]{1,0:T(8,128)(2,1)}), bf16[2048,1408]{1,0:T(8,128)(2,1)}) %all-gather.12.cloned.1.call-update) | async-done | bytes 5767184 | tf_op jit(solution)/shard_map/all_gather | solution.py:144
  142.0 34.2 %all-gather.10.cloned.1.call-done = bf16[1024,2048]{1,0:T(8,128)(2,1)} async-done(((bf16[256,2048]{1,0:T(8,128)(2,1)}), bf16[1024,2048]{1,0:T(8,128)(2,1)}) %all-gather.10.cloned.1.call-update) | async-done | bytes 4194320 | tf_op jit(solution)/shard_map/all_gather | solution.py:140
  176.3 11.7 %fusion.52 = f32[1024,1408]{1,0:T(8,128)} fusion(bf16[1024,2048]{1,0:T(8,128)(2,1)} %all-gather.10.cloned.1.call-done, bf16[2048,1408]{1,0:T(8,128)(2,1)} %all-gather.12.cloned.1.call-done), kind=kOutput, calls=%fused_computation.97 | convolution fusion | flops 5905580032 | bytes 15728640 | tf_op jit(solution)/shard_map/dot_general | solution.py:142
  188.0 82.7 %all-gather.14.cloned.1.call-done = bf16[2048,1408]{1,0:T(8,128)(2,1)} async-done(((bf16[256,1408]{1,0:T(8,128)(2,1)}), bf16[2048,1408]{1,0:T(8,128)(2,1)}) %all-gather.14.cloned.1.call-update) | async-done | bytes 5767184 | tf_op jit(solution)/shard_map/all_gather | solution.py:148
  270.7 93.2 %all-gather.16.cloned.1.call-done = bf16[1408,2048]{1,0:T(8,128)(2,1)} async-done(((bf16[1408,256]{1,0:T(8,128)(2,1)}), bf16[1408,2048]{1,0:T(8,128)(2,1)}) %all-gather.16.cloned.1.call-update) | async-done | bytes 5767184 | tf_op jit(solution)/shard_map/all_gather | solution.py:150
  363.9 20.5 %convolution_convert_fusion = bf16[1024,2048]{1,0:T(8,128)(2,1)} fusion(bf16[1408,2048]{1,0:T(8,128)(2,1)} %all-gather.16.cloned.1.call-done, f32[1024,1408]{1,0:T(8,128)} %fusion.52, bf16[1024,2048]{1,0:T(8,128)(2,1)} %all-gather.10.cloned.1.call-done, bf16[2048,1408]{1,0:T(8,128)(2,1)} %all-gather.14.cloned.1.call-done), kind=kOutput, calls=%fused_computation.38 | convolution fusion | flops 11821907968 | bytes 25690112 | tf_op jit(solution)/shard_map/dot_general | solution.py:153
  384.5 42.9 %reduce-scatter.2.cloned.1.call-done = bf16[256,2048]{1,0:T(8,128)(2,1)} async-done(((bf16[1024,2048]{1,0:T(8,128)(2,1)}), bf16[256,2048]{1,0:T(8,128)(2,1)}) %reduce-scatter.2.cloned.1.call-update) | async-done | bytes 1048592 | tf_op jit(solution)/shard_map/reduce_scatter | solution.py:152
  427.4 1.5 fusion.29
  428.9 2.6 fusion.34
  (56 shorter events, 0.8 us)
Async XLA Ops:
  6.5 25.8 %copy-start.5 = (bf16[1024,256]{1,0:T(8,128)(2,1)S(1)}, bf16[1024,256]{1,0:T(8,128)(2,1)}, u32[]{:S(2)}) copy-start(bf16[1024,256]{1,0:T(8,128)(2,1)} %param.19) | copy-start | bytes 1572868
  6.5 26.0 %copy-start.6 = (bf16[1024,256]{1,0:T(8,128)(2,1)S(1)}, bf16[1024,256]{1,0:T(8,128)(2,1)}, u32[]{:S(2)}) copy-start(bf16[1024,256]{1,0:T(8,128)(2,1)} %param.20) | copy-start | bytes 1572868
  6.5 26.1 %copy-start.1 = (bf16[1024,256]{1,0:T(8,128)(2,1)S(1)}, bf16[1024,256]{1,0:T(8,128)(2,1)}, u32[]{:S(2)}) copy-start(bf16[1024,256]{1,0:T(8,128)(2,1)} %param.18) | copy-start | bytes 1572868
  6.5 85.0 %all-gather.8.cloned.1.call-start = ((), (), s32[]{:S(2)}) async-start(), calls=%async_computation.2 | async-start | bytes 5242880 | tf_op jit(solution)/shard_map/all_gather | solution.py:127
  7.3 25.5 %copy-start.7 = (f32[1024,2]{0,1:T(2,128)S(1)}, f32[1024,2]{0,1:T(2,128)}, u32[]{:S(2)}) copy-start(f32[1024,2]{0,1:T(2,128)} %param.22) | copy-start | bytes 24580
  7.3 134.8 %all-gather.12.cloned.1.call-start = ((), (), s32[]{:S(2)}) async-start(), calls=%async_computation.4 | async-start | bytes 6488064 | tf_op jit(solution)/shard_map/all_gather | solution.py:144
  8.0 168.3 %all-gather.10.cloned.1.call-start = ((), (), s32[]{:S(2)}) async-start(), calls=%async_computation.3 | async-start | bytes 5242880 | tf_op jit(solution)/shard_map/all_gather | solution.py:140
  42.4 2.6 copy-start.4
  45.0 33.4 %copy-start.2 = (bf16[1024,256]{1,0:T(8,128)(2,1)S(1)}, bf16[1024,256]{1,0:T(8,128)(2,1)}, u32[]{:S(2)}) copy-start(bf16[1024,256]{1,0:T(8,128)(2,1)} %param.18) | copy-start | bytes 1572868
  78.3 0.9 copy-start.11
  91.5 3.5 copy-start
  95.5 1.2 copy-start.3
  95.5 1.2 copy-start.8
  96.4 1.1 copy-start.9
  98.7 171.9 %all-gather.14.cloned.1.call-start = ((), (), s32[]{:S(2)}) async-start(), calls=%async_computation.5 | async-start | bytes 6488064 | tf_op jit(solution)/shard_map/all_gather | solution.py:148
  99.3 264.6 %all-gather.16.cloned.1.call-start = ((), (), s32[]{:S(2)}) async-start(), calls=%async_computation.6 | async-start | bytes 6488064 | tf_op jit(solution)/shard_map/all_gather | solution.py:150
  99.9 327.5 %reduce-scatter.2.cloned.1.call-start = ((), (), s32[]{:S(2)}) async-start(), calls=%async_computation.7 | async-start | bytes 5242880 | tf_op jit(solution)/shard_map/reduce_scatter | solution.py:152
  384.4 44.5 %copy-start.10 = (f32[2048]{0:T(1024)S(1)}, f32[2048]{0:T(1024)}, u32[]{:S(2)}) copy-start(f32[2048]{0:T(1024)} %param.31) | copy-start | bytes 24580
Sparse Core Ops, SparseCore 0:
  8.9 37.1 all-gather.7
  48.3 93.7 all-gather.11
  143.6 32.6 all-gather.9
  178.3 92.3 all-gather.13
  272.6 91.2 all-gather.15
  384.6 42.7 reduce-scatter.1
where the time goes:
time: 439 us; the launch traced here: 438 us
  waiting for transfers between devices  297 us (68%)
  blocking collectives  66.8 us (15%)
  matrix products  43.3 us (10%)
  between operations  13.8 us (3%)
  other arithmetic  9.76 us (2%)
  local copies, waits for them, and re-layouts  6.82 us (2%)
    all_gather x1, waiting for transfers between devices, per_device(): down_full = lax.all_gather(w_down, 'sp', axis=1, tiled=True)  93.2 us
    all_gather x1, waiting for transfers between devices, per_device(): lax.all_gather(w_up, 'sp', axis=0, tiled=True)  82.7 us
    all_gather x2, blocking collectives, entering(): lax.all_gather(a.astype(kind), axis)  55.4 us
    reduce_scatter x1, waiting for transfers between devices, per_device(): lax.psum_scatter(jnp.dot(hidden, down_full, preferred_element_type=jnp.fl...  42.9 us
    all_gather x1, waiting for transfers between devices, per_device(): lax.all_gather(w_gate, 'sp', axis=0, tiled=True)  41.9 us
    all_gather x1, waiting for transfers between devices, per_device(): gathered = lax.all_gather(ffn_input, 'tp', axis=0, tiled=True)  34.2 us
    dot_general x1, matrix products, per_device(): jnp.dot(hidden, down_full, preferred_element_type=jnp.float32)  20.5 us
    dot_general x1, matrix products, per_device(): jnp.dot(columns, lax.all_gather(w_gate, 'sp', axis=0, tiled=True), prefer...  11.7 us
  transfers between devices with their start and end apart: 6, of which 5 were waited for; matrix products, arithmetic and copies ran while one was open for 8% of the time, Pallas kernels for 0%

commit v1 on v0

--- a/solution.py
+++ b/solution.py
@@ -147,7 +147,12 @@
     up_act = jnp.dot(
         columns, lax.all_gather(w_up, "sp", axis=0, tiled=True), preferred_element_type=jnp.float32
     )
-    down_full = lax.all_gather(w_down, "sp", axis=1, tiled=True)
+    ring = [w_down]
+    for hop in range(7):
+        ring.append(lax.ppermute(ring[-1], "sp", [(dev, (dev + 1) % 8) for dev in range(8)]))
+    down_full = jnp.roll(
+        jnp.concatenate(ring[::-1], axis=1), (lax.axis_index("sp") + 1) * ring[0].shape[1], axis=1
+    )
     hidden = (jax.nn.silu(gate_act) * up_act).astype(jnp.bfloat16)
     branch = lax.psum_scatter(
         jnp.dot(hidden, down_full, preferred_element_type=jnp.float32)

time: 439 us -> 424 us (0.966)
  waiting for transfers between devices: 297 us -> 253 us
  local copies, waits for them, and re-layouts: 6.82 us -> 36.7 us
    ppermute x0 -> x7, waiting for transfers between devices: none -> 203 us  [per_device(): lax.ppermute(ring[-1], 'sp', [(dev, (dev + 1) % 8) for dev in range(8)])]
    all_gather x1 -> x0, waiting for transfers between devices: 93.2 us -> none  [per_device(): down_full = lax.all_gather(w_down, 'sp', axis=1, tiled=True)]
    all_gather x1, waiting for transfers between devices: 82.7 us -> 0.01 us  [per_device(): lax.all_gather(w_up, 'sp', axis=0, tiled=True)]
    all_gather x1, waiting for transfers between devices: 41.9 us -> 0.01 us  [per_device(): lax.all_gather(w_gate, 'sp', axis=0, tiled=True)]
    all_gather x1, waiting for transfers between devices: 34.2 us -> 0.01 us  [per_device(): gathered = lax.all_gather(ffn_input, 'tp', axis=0, tiled=True)]
    unnamed x26 -> x51, local copies, waits for them, and re-layouts: 1.16 us -> 24 us
    reduce_scatter x1, waiting for transfers between devices: 42.9 us -> 48.6 us  [per_device(): lax.psum_scatter(jnp.dot(hidden, down_full, preferred_element_type=jnp.fl...]
  transfers between devices with their start and end apart: 6 -> 12, of which waited for: 5 -> 8; matrix products, arithmetic and copies ran while one was open for 8% -> 15% of each run, Pallas kernels for 0% -> 0%
where the time goes in v1:
time: 424 us; the launch traced here: 423 us
  waiting for transfers between devices  253 us (60%)
  blocking collectives  67.2 us (16%)
  matrix products  43.2 us (10%)
  local copies, waits for them, and re-layouts  36.7 us (9%)
  between operations  13.4 us (3%)
  other arithmetic  9.77 us (2%)
    ppermute x7, waiting for transfers between devices, per_device(): lax.ppermute(ring[-1], 'sp', [(dev, (dev + 1) % 8) for dev in range(8)])  203 us
    all_gather x2, blocking collectives, entering(): lax.all_gather(a.astype(kind), axis)  56 us
    reduce_scatter x1, waiting for transfers between devices, per_device(): lax.psum_scatter(jnp.dot(hidden, down_full, preferred_element_type=jnp.fl...  48.6 us
    unnamed x51, local copies, waits for them, and re-layouts  24 us
    dot_general x1, matrix products, per_device(): jnp.dot(hidden, down_full, preferred_element_type=jnp.float32)  20.6 us
    dot_general x1, matrix products, per_device(): jnp.dot(columns, lax.all_gather(w_gate, 'sp', axis=0, tiled=True), prefer...  11.7 us
    all_to_all x1, blocking collectives, per_device(): lax.all_to_all(retained, 'tp', split_axis=0, concat_axis=1, tiled=True)  11.2 us
  transfers between devices with their start and end apart: 12, of which 8 were waited for; matrix products, arithmetic and copies ran while one was open for 15% of the time, Pallas kernels for 0%

profile of v1, /device:TPU:0, one launch (start us, length us, event | category | flops | bytes accessed | tf_op | source)
XLA Modules:
  0.0 423.3 jit_solution(6351513006068582303)
XLA Ops:
  6.5 0.7 all-gather.7.cloned.1.call-update
  7.3 0.7 all-gather.11.cloned.1.call-update
  8.1 2.2 copy.53
  10.3 1.2 reshape.172
  11.5 1.2 reshape.173
  12.8 0.6 reduce-window.16
  13.8 0.2 fusion.53
  14.0 22.3 %all-gather.1 = bf16[8,1,2]{2,1,0:T(2,128)(2,1)S(1)} all-gather(bf16[1,1,2]{2,1,0:T(2,128)(2,1)S(1)} %bitcast.144), channel_id=1, replica_groups=mesh['sp'=8,'tp'=4] {'sp'}, dimensions={0}, use_global_device_ids=true | all-gather | bytes 36 | tf_op jit(solution)/shard_map/all_gather | solution.py:13
  36.3 9.5 %while.26 = (s32[]{:T(128)}, f32[2,128,128]{2,1,0:T(8,128)S(1)}, f32[2,2,512,128]{3,2,1,0:T(8,128)}, f32[2,2,512]{2,1,0:T(2,128)S(1)}, bf16[2,2,512,128]{3,1,2,0...) while((s32[]{:T(128)}, f32[2,128,128]{2,1,0:T(8,128)S(1)}, ...), condition=%wide.region_3.4_spmd.clone, body=%wide.region_0.3_spmd.clone.sunk | while | flops 507643936 | bytes 5702008 | solution.py:107
  36.3 0.6 reduce-window.26
  37.4 0.2 constant_dynamic-slice_fusion.11
  37.6 0.4 constant_dynamic-slice_fusion.12
  38.0 1.0 fusion.72
  39.3 1.2 fusion.73
  40.5 0.5 convolution_add_fusion.2
  41.1 0.6 reduce-window.26
  42.4 0.4 constant_dynamic-slice_fusion.12
  42.8 1.0 fusion.72
  44.1 1.2 fusion.73
  45.3 0.5 convolution_add_fusion.2
  45.8 2.4 copy.57
  48.2 2.1 reshape.175
  50.5 33.7 %all-gather = bf16[16,128,128]{2,1,0:T(8,128)(2,1)S(1)} all-gather(bf16[2,128,128]{2,1,0:T(8,128)(2,1)S(1)} %convert_element_type.103), channel_id=2, replica_groups=mesh['sp'=8,'tp'=4] {'sp'}, dimensions={0}, use_global_device_ids=true | all-gather | bytes 589824 | tf_op jit(solution)/shard_map/all_gather | solution.py:13
  84.2 0.7 fusion.58
  85.1 0.4 multiply_convert_fusion.4
  85.5 0.4 convert_element_type.105
  85.9 11.2 %all_to_all.16 = bf16[4,256,256]{1,2,0:T(8,128)(2,1)S(1)} all-to-all(bf16[4,256,256]{1,2,0:T(8,128)(2,1)S(1)} %copy.62), channel_id=1, replica_groups=mesh['sp'=8,'tp'=4] {'tp'}, dimensions={0} | all-to-all | bytes 1048576 | tf_op jit(solution)/shard_map/all_to_all | solution.py:123
  97.2 1.8 fusion.29
  99.0 1.7 fusion.28
  100.8 0.5 fusion.27
  101.2 0.8 fusion.30
  102.1 0.7 fusion.36
  102.7 1.3 fusion.38
  104.2 36.8 %collective-permute-done = bf16[1408,256]{1,0:T(8,128)(2,1)S(1)} collective-permute-done((bf16[1408,256]{1,0:T(8,128)(2,1)S(1)}, bf16[1408,256]{1,0:T(8,128)(2,1)S(1)}, u32[]{:S(2)}, u32[]{:S(2)}) %collective-permute-start) | collective-permute-done | bytes 720928 | tf_op jit(solution)/shard_map/ppermute | solution.py:152
  141.0 33.8 %collective-permute-done.1 = bf16[1408,256]{1,0:T(8,128)(2,1)S(1)} collective-permute-done((bf16[1408,256]{1,0:T(8,128)(2,1)S(1)}, bf16[1408,256]{1,0:T(8,128)(2,1)S(1)}, u32[]{:S(2)}, u32[]{:S(2)}) %collective-permute-start.1) | collective-permute-done | bytes 720928 | tf_op jit(solution)/shard_map/ppermute | solution.py:152
  174.8 20.2 %collective-permute-done.2 = bf16[1408,256]{1,0:T(8,128)(2,1)S(1)} collective-permute-done((bf16[1408,256]{1,0:T(8,128)(2,1)S(1)}, bf16[1408,256]{1,0:T(8,128)(2,1)S(1)}, u32[]{:S(2)}, u32[]{:S(2)}) %collective-permute-start.2) | collective-permute-done | bytes 720928 | tf_op jit(solution)/shard_map/ppermute | solution.py:152
  195.0 0.8 copy-done.3
  195.9 19.3 %collective-permute-done.3 = bf16[1408,256]{1,0:T(8,128)(2,1)S(1)} collective-permute-done((bf16[1408,256]{1,0:T(8,128)(2,1)S(1)}, bf16[1408,256]{1,0:T(8,128)(2,1)S(1)}, u32[]{:S(2)}, u32[]{:S(2)}) %collective-permute-start.3) | collective-permute-done | bytes 720928 | tf_op jit(solution)/shard_map/ppermute | solution.py:152
  215.2 0.8 copy-done.5
  216.0 33.3 %collective-permute-done.4 = bf16[1408,256]{1,0:T(8,128)(2,1)S(1)} collective-permute-done((bf16[1408,256]{1,0:T(8,128)(2,1)S(1)}, bf16[1408,256]{1,0:T(8,128)(2,1)S(1)}, u32[]{:S(2)}, u32[]{:S(2)}) %collective-permute-start.4) | collective-permute-done | bytes 720928 | tf_op jit(solution)/shard_map/ppermute | solution.py:152
  249.3 0.9 copy-done.7
  250.2 23.2 %collective-permute-done.5 = bf16[1408,256]{1,0:T(8,128)(2,1)} collective-permute-done((bf16[1408,256]{1,0:T(8,128)(2,1)S(1)}, bf16[1408,256]{1,0:T(8,128)(2,1)}, u32[]{:S(2)}, u32[]{:S(2)}) %collective-permute-start.5) | collective-permute-done | bytes 720928 | tf_op jit(solution)/shard_map/ppermute | solution.py:152
  273.3 36.0 %collective-permute-done.6 = bf16[1408,256]{1,0:T(8,128)(2,1)} collective-permute-done((bf16[1408,256]{1,0:T(8,128)(2,1)}, bf16[1408,256]{1,0:T(8,128)(2,1)}, u32[]{:S(2)}, u32[]{:S(2)}) %collective-permute-start.6) | collective-permute-done | bytes 720928 | tf_op jit(solution)/shard_map/ppermute | solution.py:152
  309.4 2.1 constant_dynamic-update-slice_fusion.15
  311.5 2.1 constant_dynamic-update-slice_fusion.14
  313.6 2.1 constant_dynamic-update-slice_fusion.13
  315.7 2.2 constant_dynamic-update-slice_fusion.12
  317.9 0.9 constant_dynamic-update-slice_fusion.11
  318.8 1.0 constant_dynamic-update-slice_fusion.10
  319.8 1.0 constant_dynamic-update-slice_fusion.9
  320.8 1.0 constant_dynamic-update-slice_fusion.8
  321.7 2.1 constant_dynamic-update-slice_fusion.7
  323.8 2.1 constant_dynamic-update-slice_fusion.6
  325.9 1.0 constant_dynamic-update-slice_fusion.5
  326.9 0.9 constant_dynamic-update-slice_fusion.4
  327.8 1.0 constant_dynamic-update-slice_fusion.3
  328.8 1.0 constant_dynamic-update-slice_fusion.2
  329.8 1.0 constant_dynamic-update-slice_fusion.1
  330.8 1.0 constant_dynamic-update-slice_fusion
  331.7 11.7 %fusion.59 = f32[1024,1408]{1,0:T(8,128)} fusion(bf16[1024,2048]{1,0:T(8,128)(2,1)} %all-gather.9.cloned.1.call-done, bf16[2048,1408]{1,0:T(8,128)(2,1)} %all-gather.11.cloned.1.call-done), kind=kOutput, calls=%fused_computation.117 | convolution fusion | flops 5905580032 | bytes 15728640 | tf_op jit(solution)/shard_map/dot_general | solution.py:142
  343.4 20.6 %fusion.19 = bf16[1024,2048]{1,0:T(8,128)(2,1)} fusion(bf16[1408,4096]{1,0:T(8,128)(2,1)} %constant_dynamic-update-slice_fusion, s32[]{:T(128)S(6)} %select_n.25, f32[1024,1408]{1,0:T(8,128)} %fusion.59, bf16[1024,2048]{1,0:T(8,128)(2,1)} %all-gather.9.cloned.1.call-done, bf16[2048,1408]{1,0:T(8,128)(2,1)} %all-gather.13.cloned.1.call-done), kind=kOutput, calls=%fused_computation.40 | convolution fusion | flops 11821907968 | bytes 25690116 | tf_op jit(solution)/shard_map/dot_general | solution.py:158
  364.0 48.6 %reduce-scatter.2.cloned.1.call-done = bf16[256,2048]{1,0:T(8,128)(2,1)} async-done(((bf16[1024,2048]{1,0:T(8,128)(2,1)}), bf16[256,2048]{1,0:T(8,128)(2,1)}) %reduce-scatter.2.cloned.1.call-update) | async-done | bytes 1048592 | tf_op jit(solution)/shard_map/reduce_scatter | solution.py:157
  412.6 1.5 fusion.34
  414.2 2.6 fusion.39
  (93 shorter events, 3.0 us)
Async XLA Ops:
  6.5 6.1 %copy-start.9 = (bf16[1024,256]{1,0:T(8,128)(2,1)S(1)}, bf16[1024,256]{1,0:T(8,128)(2,1)}, u32[]{:S(2)}) copy-start(bf16[1024,256]{1,0:T(8,128)(2,1)} %param.18) | copy-start | bytes 1572868
  6.5 6.2 %copy-start.12 = (f32[1024,2]{0,1:T(2,128)S(1)}, f32[1024,2]{0,1:T(2,128)}, u32[]{:S(2)}) copy-start(f32[1024,2]{0,1:T(2,128)} %param.22) | copy-start | bytes 24580
  6.5 90.6 %all-gather.7.cloned.1.call-start = ((), (), s32[]{:S(2)}) async-start(), calls=%async_computation.2 | async-start | bytes 5242880 | tf_op jit(solution)/shard_map/all_gather | solution.py:127
  7.3 324.5 %all-gather.11.cloned.1.call-start = ((), (), s32[]{:S(2)}) async-start(), calls=%async_computation.4 | async-start | bytes 6488064 | tf_op jit(solution)/shard_map/all_gather | solution.py:144
  8.0 323.7 %all-gather.9.cloned.1.call-start = ((), (), s32[]{:S(2)}) async-start(), calls=%async_computation.3 | async-start | bytes 5242880 | tf_op jit(solution)/shard_map/all_gather | solution.py:140
  45.8 38.4 %copy-start.10 = (bf16[1024,256]{1,0:T(8,128)(2,1)S(1)}, bf16[1024,256]{1,0:T(8,128)(2,1)}, u32[]{:S(2)}) copy-start(bf16[1024,256]{1,0:T(8,128)(2,1)} %param.18) | copy-start | bytes 1572868
  45.8 39.3 %copy-start.1 = (f32[1024,256]{0,1:T(8,128)S(1)}, f32[1024,256]{0,1:T(8,128)}, u32[]{:S(2)}) copy-start(f32[1024,256]{0,1:T(8,128)} %copy.53) | copy-start | bytes 3145732
  45.8 39.3 %copy-start.16 = (f32[2,128]{1,0:T(2,128)S(1)}, f32[2,128]{1,0:T(2,128)}, u32[]{:S(2)}) copy-start(f32[2,128]{1,0:T(2,128)} %param.23) | copy-start | bytes 3076
  97.2 3.5 copy-start
  100.7 1.3 copy-start.11
  100.7 1.3 copy-start.13
  101.2 1.5 copy-start.14
  101.2 2.9 copy-start.2
  104.0 239.4 %all-gather.13.cloned.1.call-start = ((), (), s32[]{:S(2)}) async-start(), calls=%async_computation.5 | async-start | bytes 6488064 | tf_op jit(solution)/shard_map/all_gather | solution.py:148
  104.1 36.9 %collective-permute-start = (bf16[1408,256]{1,0:T(8,128)(2,1)S(1)}, bf16[1408,256]{1,0:T(8,128)(2,1)S(1)}, u32[]{:S(2)}, u32[]{:S(2)}) collective-permute-start(bf16[1408,256]{1,0:T(8,128)(2,1)S(1)} %copy-done.2), channel_id=1, source_target_pairs={{0,4},{4,8},{8,12},{12,16},{16,20},{20,24},{24,28},{28,0},{1,5},{5... | collective-permute-start | bytes 2162696 | tf_op jit(solution)/shard_map/ppermute | solution.py:152
  141.0 33.8 %collective-permute-start.1 = (bf16[1408,256]{1,0:T(8,128)(2,1)S(1)}, bf16[1408,256]{1,0:T(8,128)(2,1)S(1)}, u32[]{:S(2)}, u32[]{:S(2)}) collective-permute-start(bf16[1408,256]{1,0:T(8,128)(2,1)S(1)} %collective-permute-done), channel_id=1, source_target_pairs={{0,4},{4,8},{8,12},{12,16},{16,20},{20,24},{24,28},{28,0},{1,5},{5... | collective-permute-start | bytes 2162696 | tf_op jit(solution)/shard_map/ppermute | solution.py:152
  141.0 271.6 %reduce-scatter.2.cloned.1.call-start = ((), (), s32[]{:S(2)}) async-start(), calls=%async_computation.6 | async-start | bytes 5242880 | tf_op jit(solution)/shard_map/reduce_scatter | solution.py:157
  174.8 20.2 %collective-permute-start.2 = (bf16[1408,256]{1,0:T(8,128)(2,1)S(1)}, bf16[1408,256]{1,0:T(8,128)(2,1)S(1)}, u32[]{:S(2)}, u32[]{:S(2)}) collective-permute-start(bf16[1408,256]{1,0:T(8,128)(2,1)S(1)} %collective-permute-done.1), channel_id=1, source_target_pairs={{0,4},{4,8},{8,12},{12,16},{16,20},{20,24},{24,28},{28,0},{1,5},{5... | collective-permute-start | bytes 2162696 | tf_op jit(solution)/shard_map/ppermute | solution.py:152
  195.0 0.9 copy-start.3
  195.8 19.3 %collective-permute-start.3 = (bf16[1408,256]{1,0:T(8,128)(2,1)S(1)}, bf16[1408,256]{1,0:T(8,128)(2,1)S(1)}, u32[]{:S(2)}, u32[]{:S(2)}) collective-permute-start(bf16[1408,256]{1,0:T(8,128)(2,1)S(1)} %collective-permute-done.2), channel_id=1, source_target_pairs={{0,4},{4,8},{8,12},{12,16},{16,20},{20,24},{24,28},{28,0},{1,5},{5... | collective-permute-start | bytes 2162696 | tf_op jit(solution)/shard_map/ppermute | solution.py:152
  215.2 0.9 copy-start.5
  216.0 33.3 %collective-permute-start.4 = (bf16[1408,256]{1,0:T(8,128)(2,1)S(1)}, bf16[1408,256]{1,0:T(8,128)(2,1)S(1)}, u32[]{:S(2)}, u32[]{:S(2)}) collective-permute-start(bf16[1408,256]{1,0:T(8,128)(2,1)S(1)} %collective-permute-done.3), channel_id=1, source_target_pairs={{0,4},{4,8},{8,12},{12,16},{16,20},{20,24},{24,28},{28,0},{1,5},{5... | collective-permute-start | bytes 2162696 | tf_op jit(solution)/shard_map/ppermute | solution.py:152
  249.3 0.9 copy-start.7
  250.2 23.2 %collective-permute-start.5 = (bf16[1408,256]{1,0:T(8,128)(2,1)S(1)}, bf16[1408,256]{1,0:T(8,128)(2,1)}, u32[]{:S(2)}, u32[]{:S(2)}) collective-permute-start(bf16[1408,256]{1,0:T(8,128)(2,1)S(1)} %collective-permute-done.4), channel_id=1, source_target_pairs={{0,4},{4,8},{8,12},{12,16},{16,20},{20,24},{24,28},{28,0},{1,5},{5... | collective-permute-start | bytes 2162696 | tf_op jit(solution)/shard_map/ppermute | solution.py:152
  273.3 36.0 %collective-permute-start.6 = (bf16[1408,256]{1,0:T(8,128)(2,1)}, bf16[1408,256]{1,0:T(8,128)(2,1)}, u32[]{:S(2)}, u32[]{:S(2)}) collective-permute-start(bf16[1408,256]{1,0:T(8,128)(2,1)} %collective-permute-done.5), channel_id=1, source_target_pairs={{0,4},{4,8},{8,12},{12,16},{16,20},{20,24},{24,28},{28,0},{1,5},{5... | collective-permute-start | bytes 2162696 | tf_op jit(solution)/shard_map/ppermute | solution.py:152
  273.3 44.6 %copy-start.4 = (bf16[1408,256]{1,0:T(8,128)(2,1)S(1)}, bf16[1408,256]{1,0:T(8,128)(2,1)}, u32[]{:S(2)}) copy-start(bf16[1408,256]{1,0:T(8,128)(2,1)} %copy-done.3) | copy-start | bytes 2162692
  313.6 12.3 %copy-start.8 = (bf16[1408,256]{1,0:T(8,128)(2,1)S(1)}, bf16[1408,256]{1,0:T(8,128)(2,1)}, u32[]{:S(2)}) copy-start(bf16[1408,256]{1,0:T(8,128)(2,1)} %copy-done.7) | copy-start | bytes 2162692
  315.7 11.2 %copy-start.6 = (bf16[1408,256]{1,0:T(8,128)(2,1)S(1)}, bf16[1408,256]{1,0:T(8,128)(2,1)}, u32[]{:S(2)}) copy-start(bf16[1408,256]{1,0:T(8,128)(2,1)} %copy-done.5) | copy-start | bytes 2162692
  343.4 70.8 %copy-start.15 = (f32[2048]{0:T(1024)S(1)}, f32[2048]{0:T(1024)}, u32[]{:S(2)}) copy-start(f32[2048]{0:T(1024)} %param.31) | copy-start | bytes 24580
Sparse Core Ops, SparseCore 0:
  8.9 37.1 all-gather.6
  48.3 109.3 all-gather.10
  159.2 48.7 all-gather.8
  210.1 125.8 all-gather.12
  364.1 48.4 reduce-scatter.1
